TPU v7x, 32 devices: a whole 2x2x4 slice. The times are simulated.
32 devices in a mesh: sp: 16 (over z, y, x), tp: 2 (over core).
Axes of the slice: x: 2, y: 2, z: 4, core: 2. Of those that a mesh axis runs over, the one named last changes fastest.
Arguments:
- queries: bfloat16 [4096, 1024], P('sp', 'tp'), may hold values from -100 to 100
- keys: bfloat16 [256, 4096], P('tp', 'sp'), may hold values from -5 to 5
- values: bfloat16 [256, 4096], P('tp', 'sp'), may hold values from -4.5 to 4.5
- gate_cache: float32 [8, 4096], P('tp', 'sp'), as said below
- documents: int32 [4096], P('sp'), may hold values from 0 to 2, never falling along the last dimension, each value on 1 to 2560 neighbouring positions
- residual: bfloat16 [4096, 2048], P(('sp', 'tp')), may hold values from -3 to 3
- out_weight: bfloat16 [1024, 2048], replicated, may hold values from -2 to 2
- mix_gain: bfloat16 [2048], replicated, may hold values from 0.099609375 to 1.8984375
- routes: int32 [4096, 4], P(('sp', 'tp')), may hold values from 0 to 31, all different within a row; in each aligned block of 128 rows (0 to 127, 128 to 255, ...) at most 32 rows name the same one
- route_weight: float32 [4096, 4], P(('sp', 'tp')), may hold values from 0.25 to 1
- expert_gate: bfloat16 [32, 2048, 512], P(('sp', 'tp')), may hold values from -0.125 to 0.125
- expert_up: bfloat16 [32, 2048, 512], P(('sp', 'tp')), may hold values from -0.125 to 0.125
- expert_down: bfloat16 [32, 512, 2048], P(('sp', 'tp')), may hold values from -0.25 to 0.25
- shared_gate: bfloat16 [2048, 512], replicated, may hold values from -0.125 to 0.125
- shared_up: bfloat16 [2048, 512], replicated, may hold values from -0.125 to 0.125
- shared_down: bfloat16 [512, 2048], replicated, may hold values from -0.25 to 0.25
- ffn_gain: bfloat16 [2048], replicated, may hold values from 0.099609375 to 1.8984375
Outputs:
- result: bfloat16 [4096, 2048], P(('sp', 'tp'))
Inputs may be any that keep to these rules, and one draw needn't show every extreme that they name: `gate_cache`: entry (h, j) is the sum of head h's log forget gates over positions 0 to j. `documents`: never falls along the positions; no document has more than 2560 positions. `routes`: each row names 4 different experts; in the rows of one device (aligned blocks of 128 rows) no expert is named more than 32 times, a bound that some block reaches.
All inputs are finite; a program needn't handle non-finite values.
Results may differ from a plain program's by a relative error of at most 0.013.
Values may be sent and summed in bfloat16 or wider, within the bound.
A program may use at most 256 MiB of HBM per device.

v0:
```python
import jax
import jax.numpy as jnp
from jax import lax
from jax.sharding import PartitionSpec as P

HD = 128


residual_scale = 2.0**0.25
norm_epsilon = 1e-05
masked_score = -1e30


def normalize(summed, gain_vector):
    row_mean = jnp.mean(summed, axis=-1, keepdims=True)
    centred = summed - row_mean
    spread = jnp.mean(centred * centred, axis=-1, keepdims=True)
    return (centred * lax.rsqrt(spread + norm_epsilon) * gain_vector.astype(jnp.float32)).astype(
        jnp.bfloat16
    )


def expert_block(arrived, expert_gate, expert_up, expert_down):
    own_count = expert_gate.shape[0]
    grouped = arrived.reshape(-1, own_count, arrived.shape[1], arrived.shape[2])
    gate_part = jnp.einsum(
        "nemd,edf->nemf", grouped, expert_gate, preferred_element_type=jnp.float32
    )
    up_part = jnp.einsum("nemd,edf->nemf", grouped, expert_up, preferred_element_type=jnp.float32)
    hidden = (jax.nn.silu(gate_part) * up_part).astype(jnp.bfloat16)
    produced = jnp.einsum("nemf,efd->nemd", hidden, expert_down, preferred_element_type=jnp.float32)
    return produced.astype(jnp.bfloat16).reshape(arrived.shape)


def local(
    queries,
    keys,
    values,
    gate_cache,
    documents,
    residual,
    out_weight,
    mix_gain,
    routes,
    route_weight,
    expert_gate,
    expert_up,
    expert_down,
    shared_gate,
    shared_up,
    shared_down,
    ffn_gain,
):
    tok_rows = queries.shape[0]
    local_heads = gate_cache.shape[0]
    kv_local = keys.shape[0] // HD
    group_size = local_heads // kv_local
    score_scale = HD ** (-0.5)
    seq_start = lax.axis_index("sp") * tok_rows
    query_pos = seq_start + jnp.arange(tok_rows, dtype=jnp.int32)
    query_last = seq_start + tok_rows - 1
    query_cum = jnp.transpose(gate_cache).reshape(tok_rows, kv_local, group_size)
    grouped_q = queries.reshape(tok_rows, kv_local, group_size, HD)
    all_cache, all_docs = (
        lax.all_gather(gate_cache, "sp", axis=1, tiled=True),
        lax.all_gather(documents.reshape(1, tok_rows), "sp", axis=1, tiled=True),
    )
    doc_line = all_docs[0]
    initial = (
        jnp.full((tok_rows, kv_local, group_size), masked_score, jnp.float32),
        jnp.zeros((tok_rows, kv_local, group_size), jnp.float32),
        jnp.zeros((tok_rows, kv_local, group_size, HD), jnp.float32),
    )
    key_piece = lax.all_gather(keys, "sp", axis=1, tiled=True)
    value_piece = lax.all_gather(values, "sp", axis=1, tiled=True)
    width_keys = key_piece.shape[1]
    key_cum = all_cache.reshape(kv_local, group_size, width_keys)

    def update(state):
        running_max, running_sum, numerator = state
        key_block = key_piece.reshape(kv_local, HD, width_keys)
        value_block = value_piece.reshape(kv_local, HD, width_keys)
        scores = (
            jnp.einsum("qagd,adk->qagk", grouped_q, key_block, preferred_element_type=jnp.float32)
            * score_scale
        )
        scores = scores + query_cum[..., None] - key_cum[None]
        key_pos = jnp.arange(width_keys, dtype=jnp.int32)
        allowed = (key_pos[None, :] <= query_pos[:, None]) & (
            doc_line[None, :] == documents[:, None]
        )
        allowed = allowed[:, None, None, :]
        scores = jnp.where(allowed, scores, masked_score)
        new_max = jnp.maximum(running_max, jnp.max(scores, axis=-1))
        weights = jnp.where(allowed, jnp.exp(scores - new_max[..., None]), 0.0)
        new_sum = jnp.sum(weights, axis=-1)
        added = jnp.einsum(
            "qagk,adk->qagd",
            weights.astype(jnp.bfloat16),
            value_block,
            preferred_element_type=jnp.float32,
        )
        return (new_max, new_sum, added)

    active = (jnp.int32(0) <= query_last) & (doc_line[width_keys - 1] >= documents[0])
    running_max, running_sum, numerator = lax.cond(active, update, lambda state: state, initial)
    attended = (
        (numerator / running_sum[..., None])
        .astype(jnp.bfloat16)
        .reshape(tok_rows, local_heads * HD)
    )
    token_heads = lax.all_to_all(attended, "tp", split_axis=0, concat_axis=1, tiled=True)
    mixed = jnp.dot(token_heads, out_weight, preferred_element_type=jnp.float32)
    mixed = lax.optimization_barrier(mixed.astype(jnp.bfloat16)).astype(jnp.float32)
    settled = normalize(residual_scale * residual.astype(jnp.float32) + mixed, mix_gain)
    row_count = settled.shape[0]
    width_model = settled.shape[1]
    top_count = routes.shape[1]
    expert_total = lax.axis_size(("sp", "tp")) * expert_gate.shape[0]
    capacity = row_count * lax.axis_size("tp") * top_count // expert_total
    chosen_experts = routes.reshape(-1)
    matches = (
        chosen_experts[:, None] == jnp.arange(expert_total, dtype=jnp.int32)[None, :]
    ).astype(jnp.int32)
    ranks = jnp.sum(jnp.cumsum(matches, axis=0) * matches, axis=1) - 1
    slots = chosen_experts * capacity + ranks
    placing = slots[None, :] == jnp.arange(expert_total * capacity, dtype=jnp.int32)[:, None]
    placing = jnp.any(
        placing.reshape(expert_total * capacity, row_count, top_count), axis=2
    ).astype(jnp.bfloat16)
    outgoing = jnp.dot(placing, settled, preferred_element_type=jnp.float32).astype(jnp.bfloat16)
    outgoing = outgoing.reshape(expert_total, capacity, width_model)
    finished = expert_block(
        lax.all_to_all(outgoing, ("sp", "tp"), split_axis=0, concat_axis=0, tiled=True),
        expert_gate,
        expert_up,
        expert_down,
    )
    returned = lax.all_to_all(finished, ("sp", "tp"), split_axis=0, concat_axis=0, tiled=True)
    returned = returned.reshape(expert_total * capacity, width_model)
    picked_rows = jnp.take(returned, slots, axis=0).reshape(row_count, top_count, width_model)
    routed = jnp.einsum("rkd,rk->rd", picked_rows.astype(jnp.float32), route_weight)
    shared_gate_part = jnp.dot(settled, shared_gate, preferred_element_type=jnp.float32)
    shared_up_part = jnp.dot(settled, shared_up, preferred_element_type=jnp.float32)
    shared_hidden = (jax.nn.silu(shared_gate_part) * shared_up_part).astype(jnp.bfloat16)
    shared = jnp.dot(shared_hidden, shared_down, preferred_element_type=jnp.float32)
    return normalize(residual_scale * settled.astype(jnp.float32) + routed + shared, ffn_gain)


def solution(mesh):
    placed = (
        P("sp", "tp"),
        P("tp", "sp"),
        P("tp", "sp"),
        P("tp", "sp"),
        P("sp"),
        P(("sp", "tp"), None),
        P(),
        P(),
        P(("sp", "tp"), None),
        P(("sp", "tp"), None),
        P(("sp", "tp"), None, None),
        P(("sp", "tp"), None, None),
        P(("sp", "tp"), None, None),
        P(),
        P(),
        P(),
        P(),
    )
    return jax.shard_map(
        local, mesh=mesh, in_specs=placed, out_specs=P(("sp", "tp"), None), check_vma=False
    )
```

profile of v0, /device:TPU:0, one launch (start us, length us, event | category | flops | bytes accessed | tf_op | source)
XLA Modules:
  0.0 393.6 jit_solution(2535516395564024456)
XLA Ops:
  6.5 1.7 copy.56
  8.3 0.7 all-gather.7.cloned.1.call-update
  9.0 0.8 copy.59
  10.1 1.2 slice.14
  11.3 42.7 %all-gather.1 = s32[16,1,256]{2,1,0:T(1,128)S(1)} all-gather(s32[1,1,256]{2,1,0:T(1,128)} %bitcast.172), channel_id=2, replica_groups=mesh['sp'=16,'tp'=2] {'sp'}, dimensions={0}, use_global_device_ids=true | all-gather | bytes 17408 | tf_op jit(solution)/shard_map/all_gather | solution.py:66
  54.0 0.6 slice.19
  55.8 0.7 convert_element_type.60
  56.5 1.2 reduce-window.6
  58.3 36.1 %all_gather.14 = f32[4,4096]{1,0:T(4,128)S(1)} all-gather(f32[4,256]{1,0:T(4,128)} %param.22), channel_id=1, replica_groups=mesh['sp'=16,'tp'=2] {'sp'}, dimensions={1}, use_global_device_ids=true | all-gather | bytes 69632 | tf_op jit(solution)/shard_map/all_gather | solution.py:65
  94.4 0.7 compare_and_fusion
  95.1 0.4 fusion.31
  95.4 29.3 %all-gather.7.cloned.1.call-done = bf16[128,4096]{1,0:T(8,128)(2,1)} async-done(((bf16[128,256]{1,0:T(8,128)(2,1)}), bf16[128,4096]{1,0:T(8,128)(2,1)}) %all-gather.7.cloned.1.call-update) | async-done | bytes 1048592 | tf_op jit(solution)/shard_map/all_gather | solution.py:75
  124.7 20.7 %conditional.1 = (f32[256,1,4]{0,2,1:T(4,128)S(1)}, f32[256,1,4,128]{3,0,2,1:T(8,128)S(1)}) conditional(s32[]{:T(128)} %convert_element_type.56, () %tuple.13, (s32[]{:T(128)}, s32[256]{0:T(256)S(1)}, s32[1,4096]{1,0:T(1,128)S(1)}, s32[256]{0:T(256)}, bf16[256,512]{1,0:T(8,128)(2,1)}, /*index=5*/bf16[128,4096]{0,1:T(8,128)(2,1)}, f32[256,4]{0,1:T(4,128)}, ...), branch_computations={%region_0.0_spmd, %region_1.4_spmd} | conditional | flops 2230320384 | bytes 61874252 | solution.py:106
  124.7 2.5 fusion.8
  127.3 5.5 %fusion.3 = (f32[256,4]{0,1:T(4,128)S(1)}, f32[4096,256,4]{1,0,2:T(8,128)S(1)}) fusion(f32[4,4096]{1,0:T(4,128)S(1)} %get-tuple-element.33, f32[256,4]{0,1:T(4,128)} %get-tuple-element.32, pred[256,4096]{0,1:T(8,128)(4,1)S(1)} %fusion.8, bf16[128,4096]{0,1:T(8,128)(2,1)} %get-tuple-element.30, bf16[256,512]{1,0:T(8,128)(2,1)} %get-tuple-element.40), kind=kOutput, calls=%fused_computation.7 | convolution fusion | flops 1094712320 | bytes 19210240 | tf_op jit(solution)/shard_map/cond/branch_1_fun/qagd,adk->qagk/dot_general | solution.py:84
  132.8 6.8 %fusion.9 = f32[256,1,4,128]{3,0,2,1:T(8,128)S(1)} fusion(f32[4096,256,4]{1,0,2:T(8,128)S(1)} %get-tuple-element.44, f32[256,4]{0,1:T(4,128)S(1)} %broadcast_maximum_fusion, f32[4,4096]{1,0:T(4,128)S(1)} %get-tuple-element.33, f32[256,4]{0,1:T(4,128)S(1)} %copy-done.5, pred[256,4096]{0,1:T(8,128)(4,1)S(1)} %fusion.8, bf16[128,4096]{1,0:T(8,128)(2,1)S(1)} %copy-done.9), kind=kOutput, calls=%fused_computation.13 | convolution fusion | flops 1103101952 | bytes 19472384 | tf_op jit(solution)/shard_map/cond/branch_1_fun/qagk,adk->qagd/dot_general | solution.py:97
  139.7 5.8 %fusion.2 = f32[256,4]{0,1:T(4,128)S(1)} fusion(f32[4096,256,4]{1,0,2:T(8,128)S(1)} %get-tuple-element.44, f32[256,4]{0,1:T(4,128)S(1)} %broadcast_maximum_fusion, f32[4,4096]{1,0:T(4,128)S(1)} %get-tuple-element.33, f32[256,4]{0,1:T(4,128)S(1)} %copy-done.5, pred[256,4096]{0,1:T(8,128)(4,1)S(1)} %fusion.8), kind=kLoop, calls=%fused_computation.6 | loop fusion | flops 29359104 | bytes 17903616 | tf_op jit(solution)/shard_map/cond/branch_1_fun/reduce_sum | solution.py:96
  146.0 3.9 %all_to_all.29 = bf16[2,128,512]{2,1,0:T(8,128)(2,1)S(1)} all-to-all(bf16[2,128,512]{2,1,0:T(8,128)(2,1)S(1)} %all_to_all.20), channel_id=1, replica_groups=mesh['sp'=16,'tp'=2] {'tp'}, dimensions={0} | all-to-all | bytes 524288 | tf_op jit(solution)/shard_map/all_to_all | solution.py:112
  150.1 2.9 convolution_convert_fusion.2
  154.0 1.2 convolution_convert_fusion.1
  155.2 96.7 %all_to_all.30 = bf16[32,32,2048]{2,1,0:T(8,128)(2,1)S(1)} all-to-all(bf16[32,32,2048]{2,1,0:T(8,128)(2,1)S(1)} %bitcast.161), channel_id=1, replica_groups=mesh['sp'=16,'tp'=2] {'sp','tp'}, dimensions={0} | all-to-all | bytes 8388608 | tf_op jit(solution)/shard_map/all_to_all | solution.py:134
  252.0 2.0 copy-done.3
  253.9 3.7 fusion.22
  257.7 10.1 %convolution_convert_fusion = bf16[32,32,2048]{2,1,0:T(8,128)(2,1)} fusion(bf16[1,512,2048]{2,1,0:T(8,128)(2,1)S(1)} %copy-done, f32[32,32,512]{2,1,0:T(8,128)} %fusion.22, bf16[32,32,2048]{2,1,0:T(8,128)(2,1)} %copy-done.3, bf16[1,2048,512]{2,1,0:T(8,128)(2,1)} %param.29), kind=kOutput, calls=%fused_computation.24 | convolution fusion | flops 4300210176 | bytes 14680064 | tf_op jit(solution)/shard_map/nemf,efd->nemd/dot_general | solution.py:31
  267.7 4.0 %all-to-all-start.2 = ((bf16[32,32,2048]{2,1,0:T(8,128)(2,1)}), bf16[32,32,2048]{2,1,0:T(8,128)(2,1)}, u32[]{:S(2)}, u32[]{:S(2)}) async-start(bf16[32,32,2048]{2,1,0:T(8,128)(2,1)} %convolution_convert_fusion), calls=%async_computation.2 | async-start | bytes 8388608 | tf_op jit(solution)/shard_map/all_to_all | solution.py:139
  272.4 2.0 fusion.58
  274.4 91.0 %all-to-all-done.2 = bf16[32,32,2048]{2,1,0:T(8,128)(2,1)} async-done(((bf16[32,32,2048]{2,1,0:T(8,128)(2,1)}), bf16[32,32,2048]{2,1,0:T(8,128)(2,1)}, u32[]{:S(2)}, u32[]{:S(2)}) %all-to-all-start.2) | async-done | bytes 4194336 | tf_op jit(solution)/shard_map/all_to_all | solution.py:139
  365.5 8.0 %gather_fusion = bf16[512,2048]{1,0:T(8,128)(2,1)} fusion(bf16[1024,2048]{1,0:T(8,128)(2,1)} %bitcast.35, s32[1024]{0:T(1024)S(1)} %pad_clamp_fusion), kind=kCustom, calls=%fused_computation | custom fusion | bytes 4196352 | tf_op jit(solution)/shard_map/jit(_take)/gather | solution.py:141
  373.5 4.1 %gather.7 = bf16[128,4,2048]{2,1,0:T(4,128)(2,1)} reshape(bf16[512,2048]{1,0:T(8,128)(2,1)} %gather_fusion) | data formatting | bytes 4194304 | tf_op jit(solution)/shard_map/jit(_take)/gather | solution.py:141
  377.6 3.9 fusion.29
  381.5 4.0 %fusion.57 = (f32[128]{0:T(128)S(1)}, f32[128,2048]{1,0:T(8,128)S(1)}) fusion(bf16[512,2048]{1,0:T(8,128)(2,1)} %param.34, bf16[128,2048]{1,0:T(8,128)(2,1)} %copy-done.1, bf16[2048,512]{1,0:T(8,128)(2,1)} %param.33, f32[128,512]{1,0:T(8,128)S(1)} %fusion.58, f32[128,1,2048]{2,1,0:T(1,128)} %fusion.29), kind=kOutput, calls=%fused_computation.85 | convolution fusion | flops 538574720 | bytes 7078400 | tf_op jit(solution)/shard_map/dot_general | solution.py:146
  385.7 1.0 multiply_convert_fusion
  (56 shorter events, 3.3 us)
Async XLA Ops:
  6.5 251.1 %copy-start = (bf16[1,512,2048]{2,1,0:T(8,128)(2,1)S(1)}, bf16[1,512,2048]{2,1,0:T(8,128)(2,1)}, u32[]{:S(2)}) copy-start(bf16[1,512,2048]{2,1,0:T(8,128)(2,1)} %param.31) | copy-start | bytes 6291460
  6.5 88.9 %all-gather.5.cloned.1.call-start = ((), (), s32[]{:S(2)}) async-start(), calls=%async_computation.3 | async-start | bytes 1114112 | tf_op jit(solution)/shard_map/all_gather | solution.py:74
  8.3 116.4 %all-gather.7.cloned.1.call-start = ((), (), s32[]{:S(2)}) async-start(), calls=%async_computation.4 | async-start | bytes 1114112 | tf_op jit(solution)/shard_map/all_gather | solution.py:75
  127.3 5.5 %copy-start.5 = (f32[256,4]{0,1:T(4,128)S(1)}, f32[256,4]{0,1:T(4,128)}, u32[]{:S(2)}) copy-start(f32[256,4]{0,1:T(4,128)} %get-tuple-element.32) | copy-start | bytes 12292 | tf_op jit(solution)/shard_map/cond
  127.3 5.5 %copy-start.9 = (bf16[128,4096]{1,0:T(8,128)(2,1)S(1)}, bf16[128,4096]{1,0:T(8,128)(2,1)}, u32[]{:S(2)}) copy-start(bf16[128,4096]{1,0:T(8,128)(2,1)} %get-tuple-element.34) | copy-start | bytes 3145732 | tf_op jit(solution)/shard_map/cond
  145.5 7.6 %copy-start.2 = (bf16[128,2048]{1,0:T(8,128)(2,1)S(1)}, bf16[128,2048]{1,0:T(8,128)(2,1)}, u32[]{:S(2)}) copy-start(bf16[128,2048]{1,0:T(8,128)(2,1)} %param.24) | copy-start | bytes 1572868
  154.0 118.4 %copy-start.1 = (bf16[128,2048]{1,0:T(8,128)(2,1)}, bf16[128,2048]{1,0:T(8,128)(2,1)S(1)}, u32[]{:S(2)}) copy-start(bf16[128,2048]{1,0:T(8,128)(2,1)S(1)} %multiply_convert_fusion.1) | copy-start | bytes 1572868
  155.2 98.7 %copy-start.8 = (bf16[1,2048,512]{2,1,0:T(8,128)(2,1)S(1)}, bf16[1,2048,512]{2,1,0:T(8,128)(2,1)}, u32[]{:S(2)}) copy-start(bf16[1,2048,512]{2,1,0:T(8,128)(2,1)} %param.30) | copy-start | bytes 6291460
  252.0 2.0 copy-start.3
  267.7 4.0 %copy-start.4 = (s32[128,4]{0,1:T(4,128)S(1)}, s32[128,4]{0,1:T(4,128)}, u32[]{:S(2)}) copy-start(s32[128,4]{0,1:T(4,128)} %param.27) | copy-start | bytes 6148
  267.7 4.4 %copy-start.7 = (f32[128,4]{0,1:T(4,128)S(1)}, f32[128,4]{0,1:T(4,128)}, u32[]{:S(2)}) copy-start(f32[128,4]{0,1:T(4,128)} %param.28) | copy-start | bytes 6148
  267.7 4.6 %copy-start.6 = (bf16[2048]{0:T(1024)(128)(2,1)S(1)}, bf16[2048]{0:T(1024)(128)(2,1)}, u32[]{:S(2)}) copy-start(bf16[2048]{0:T(1024)(128)(2,1)} %param.35) | copy-start | bytes 12292
  267.7 97.7 %all-to-all-start.2 = ((bf16[32,32,2048]{2,1,0:T(8,128)(2,1)}), bf16[32,32,2048]{2,1,0:T(8,128)(2,1)}, u32[]{:S(2)}, u32[]{:S(2)}) async-start(bf16[32,32,2048]{2,1,0:T(8,128)(2,1)} %convolution_convert_fusion), calls=%async_computation.2 | async-start | bytes 8388608 | tf_op jit(solution)/shard_map/all_to_all | solution.py:139
Sparse Core Ops, SparseCore 0:
  10.1 57.9 all-gather.4
  70.8 53.9 all-gather.6
where the time goes:
time: 394 us
  blocking collectives  180 us (46%)
  waiting for transfers between devices  121 us (31%)
  matrix products  40.2 us (10%)
  local copies, waits for them, and re-layouts  20.1 us (5%)
  between operations  14.9 us (4%)
  other arithmetic  13.8 us (4%)
  starting transfers between devices  4.06 us (1%)
    all_to_all x1, blocking collectives, local(): lax.all_to_all(outgoing, ('sp', 'tp'), split_axis=0, concat_axis=0, tiled...  96.7 us
    all_to_all x1, waiting for transfers between devices, local(): lax.all_to_all(finished, ('sp', 'tp'), split_axis=0, concat_axis=0, tiled...  91 us
    all_gather x1, blocking collectives, local(): lax.all_gather(documents.reshape(1, tok_rows), 'sp', axis=1, tiled=True)  42.7 us
    all_gather x1, blocking collectives, local(): lax.all_gather(gate_cache, 'sp', axis=1, tiled=True)  36.1 us
    all_gather x1, waiting for transfers between devices, local(): value_piece = lax.all_gather(values, 'sp', axis=1, tiled=True)  29.3 us
    gather x2, local copies, waits for them, and re-layouts, local(): jnp.take(returned, slots, axis=0).reshape(row_count, top_count, width_model)  12.1 us
    dot_general x1, matrix products, expert_block(): jnp.einsum('nemf,efd->nemd', hidden, expert_down, preferred_element_type=...  10.1 us
  transfers between devices with their start and end apart: 3, of which 2 were waited for; matrix products, arithmetic and copies ran while one was open for 2% of the time, Pallas kernels for 0%

commit v1 on v0

--- a/solution.py
+++ b/solution.py
@@ -1,6 +1,10 @@
+import functools
+
 import jax
 import jax.numpy as jnp
 from jax import lax
+from jax.experimental import pallas as pl
+from jax.experimental.pallas import tpu as pltpu
 from jax.sharding import PartitionSpec as P
 
 HD = 128
@@ -18,6 +22,210 @@
     return (centred * lax.rsqrt(spread + norm_epsilon) * gain_vector.astype(jnp.float32)).astype(
         jnp.bfloat16
     )
+
+
+def attend_kernel(
+    planes, across, q_ref, kv_ref, aux_ref, gate_ref, doc_ref, out_ref,
+    kv_all, aux_all, top, total, acc, own_sem, up_send, up_recv, side_send, side_recv,
+):
+    heads = gate_ref.shape[1]
+    tok_rows = q_ref.shape[0]
+    group_size = heads // (kv_ref.shape[0] // (2 * HD))
+    kv_rows = kv_ref.shape[0] // 2
+    me = lax.axis_index("sp")
+    plane = me // across
+    column = me % across
+
+    barrier = pltpu.get_barrier_semaphore()
+
+    def greet(other):
+        pl.semaphore_signal(
+            barrier, inc=1, device_id={"sp": other}, device_id_type=pl.DeviceIdType.MESH
+        )
+
+    for offset in range(1, across):
+        greet(plane * across + (column + offset) % across)
+
+    @pl.when(plane + 1 < planes)
+    def _():
+        greet(me + across)
+
+    @pl.when(plane > 0)
+    def _():
+        greet(me - across)
+
+    peers = across + 1
+    pl.semaphore_wait(
+        barrier,
+        peers - (planes - plane) // planes - (plane + 1) // planes,
+    )
+
+    def copies(slot, other, send_sem, recv_sem, index):
+        return [
+            pltpu.make_async_remote_copy(
+                src_ref=ref.at[slot],
+                dst_ref=ref.at[slot],
+                send_sem=send_sem.at[index, part],
+                recv_sem=recv_sem.at[index, part],
+                device_id={"sp": other},
+                device_id_type=pl.DeviceIdType.MESH,
+            )
+            for part, ref in enumerate((kv_all, aux_all))
+        ]
+
+    own = [
+        pltpu.make_async_copy(kv_ref, kv_all.at[me], own_sem.at[0]),
+        pltpu.make_async_copy(aux_ref, aux_all.at[me], own_sem.at[1]),
+    ]
+    for copy in own:
+        copy.start()
+    top[...] = jnp.full_like(top, masked_score)
+    total[...] = jnp.zeros_like(total)
+    acc[...] = jnp.zeros_like(acc)
+    for copy in own:
+        copy.wait()
+
+    def absorb(slot):
+        key_pos = slot * tok_rows + lax.broadcasted_iota(jnp.int32, (tok_rows, tok_rows), 1)
+        query_pos = me * tok_rows + lax.broadcasted_iota(jnp.int32, (tok_rows, tok_rows), 0)
+        allowed = (key_pos <= query_pos) & (aux_all[slot, heads : heads + 1, :] == doc_ref[...])
+        for head in range(heads):
+            base = head // group_size * HD
+            columns = slice(head * HD, (head + 1) * HD)
+            key_block = kv_all[slot, base : base + HD, :]
+            value_block = kv_all[slot, kv_rows + base : kv_rows + base + HD, :]
+            scores = jnp.dot(
+                q_ref[:, columns], key_block, preferred_element_type=jnp.float32
+            ) * (HD ** (-0.5))
+            scores = scores + (gate_ref[:, head : head + 1] - aux_all[slot, head : head + 1, :])
+            scores = jnp.where(allowed, scores, masked_score)
+            old_top = top[head]
+            new_top = jnp.maximum(old_top, jnp.max(scores, axis=1, keepdims=True))
+            weights = jnp.where(allowed, jnp.exp(scores - new_top), 0.0)
+            shrink = jnp.exp(old_top - new_top)
+            top[head] = new_top
+            total[head] = total[head] * shrink + jnp.sum(weights, axis=1, keepdims=True)
+            acc[:, columns] = acc[:, columns] * shrink + lax.dot_general(
+                weights.astype(jnp.bfloat16),
+                value_block,
+                (((1,), (1,)), ((), ())),
+                preferred_element_type=jnp.float32,
+            )
+
+    def rise(step, carry):
+        @pl.when(plane >= step)
+        def _():
+            slot = me - step * across
+
+            @pl.when(step > 0)
+            def _():
+                for copy in copies(slot, me - across, up_send, up_recv, step - 1):
+                    copy.wait_recv()
+
+            @pl.when(plane + 1 < planes)
+            def _():
+                for copy in copies(slot, me + across, up_send, up_recv, step):
+                    copy.start()
+
+            for offset in range(1, across):
+
+                @pl.when((step > 0) | (column + offset < across))
+                def _():
+                    other = plane * across + (column + offset) % across
+                    for copy in copies(
+                        slot, other, side_send, side_recv, step * across + offset
+                    ):
+                        copy.start()
+
+            absorb(slot)
+
+        return carry
+
+    lax.fori_loop(0, planes, rise, 0)
+
+    def spread(turn, carry):
+        step = turn // (across - 1)
+        offset = 1 + turn % (across - 1)
+
+        @pl.when((plane >= step) & ((step > 0) | (column >= offset)))
+        def _():
+            source = (column + across - offset) % across
+            slot = (plane - step) * across + source
+            for copy in copies(
+                slot, plane * across + source, side_send, side_recv, step * across + offset
+            ):
+                copy.wait_recv()
+            absorb(slot)
+
+        return carry
+
+    lax.fori_loop(0, planes * (across - 1), spread, 0)
+
+    def settle(step, carry):
+        @pl.when(plane >= step)
+        def _():
+            slot = me - step * across
+
+            @pl.when(plane + 1 < planes)
+            def _():
+                for copy in copies(slot, me + across, up_send, up_recv, step):
+                    copy.wait_send()
+
+            for offset in range(1, across):
+
+                @pl.when((step > 0) | (column + offset < across))
+                def _():
+                    other = plane * across + (column + offset) % across
+                    for copy in copies(
+                        slot, other, side_send, side_recv, step * across + offset
+                    ):
+                        copy.wait_send()
+
+        return carry
+
+    lax.fori_loop(0, planes, settle, 0)
+    for head in range(heads):
+        columns = slice(head * HD, (head + 1) * HD)
+        out_ref[:, columns] = (acc[:, columns] / total[head]).astype(out_ref.dtype)
+
+
+def attend(queries, keys, values, gate_cache, documents):
+    tok_rows = queries.shape[0]
+    heads = gate_cache.shape[0]
+    devices = lax.axis_size("sp")
+    planes = min(4, devices)
+    across = devices // planes
+    aux_rows = (heads + 8) // 8 * 8
+    doc_line = documents.astype(jnp.float32)
+    packed = jnp.concatenate([keys, values], axis=0)
+    aux = jnp.concatenate(
+        [
+            gate_cache,
+            jnp.broadcast_to(doc_line[None, :], (aux_rows - heads, tok_rows)),
+        ],
+        axis=0,
+    )
+    vmem = pl.BlockSpec(memory_space=pltpu.VMEM)
+    return pl.pallas_call(
+        functools.partial(attend_kernel, planes, across),
+        out_shape=jax.ShapeDtypeStruct((tok_rows, heads * HD), jnp.bfloat16),
+        in_specs=[vmem] * 5,
+        out_specs=vmem,
+        scratch_shapes=[
+            pltpu.VMEM((devices,) + packed.shape, jnp.bfloat16),
+            pltpu.VMEM((devices,) + aux.shape, jnp.float32),
+            pltpu.VMEM((heads, tok_rows, 1), jnp.float32),
+            pltpu.VMEM((heads, tok_rows, 1), jnp.float32),
+            pltpu.VMEM((tok_rows, heads * HD), jnp.float32),
+            pltpu.SemaphoreType.DMA((2,)),
+            pltpu.SemaphoreType.DMA((planes, 2)),
+            pltpu.SemaphoreType.DMA((planes, 2)),
+            pltpu.SemaphoreType.DMA((planes * across, 2)),
+            pltpu.SemaphoreType.DMA((planes * across, 2)),
+        ],
+        compiler_params=pltpu.CompilerParams(collective_id=0, has_side_effects=True),
+        name="attend",
+    )(queries, packed, aux, jnp.transpose(gate_cache), doc_line[:, None])
 
 
 def expert_block(arrived, expert_gate, expert_up, expert_down):
@@ -51,64 +259,7 @@
     shared_down,
     ffn_gain,
 ):
-    tok_rows = queries.shape[0]
-    local_heads = gate_cache.shape[0]
-    kv_local = keys.shape[0] // HD
-    group_size = local_heads // kv_local
-    score_scale = HD ** (-0.5)
-    seq_start = lax.axis_index("sp") * tok_rows
-    query_pos = seq_start + jnp.arange(tok_rows, dtype=jnp.int32)
-    query_last = seq_start + tok_rows - 1
-    query_cum = jnp.transpose(gate_cache).reshape(tok_rows, kv_local, group_size)
-    grouped_q = queries.reshape(tok_rows, kv_local, group_size, HD)
-    all_cache, all_docs = (
-        lax.all_gather(gate_cache, "sp", axis=1, tiled=True),
-        lax.all_gather(documents.reshape(1, tok_rows), "sp", axis=1, tiled=True),
-    )
-    doc_line = all_docs[0]
-    initial = (
-        jnp.full((tok_rows, kv_local, group_size), masked_score, jnp.float32),
-        jnp.zeros((tok_rows, kv_local, group_size), jnp.float32),
-        jnp.zeros((tok_rows, kv_local, group_size, HD), jnp.float32),
-    )
-    key_piece = lax.all_gather(keys, "sp", axis=1, tiled=True)
-    value_piece = lax.all_gather(values, "sp", axis=1, tiled=True)
-    width_keys = key_piece.shape[1]
-    key_cum = all_cache.reshape(kv_local, group_size, width_keys)
-
-    def update(state):
-        running_max, running_sum, numerator = state
-        key_block = key_piece.reshape(kv_local, HD, width_keys)
-        value_block = value_piece.reshape(kv_local, HD, width_keys)
-        scores = (
-            jnp.einsum("qagd,adk->qagk", grouped_q, key_block, preferred_element_type=jnp.float32)
-            * score_scale
-        )
-        scores = scores + query_cum[..., None] - key_cum[None]
-        key_pos = jnp.arange(width_keys, dtype=jnp.int32)
-        allowed = (key_pos[None, :] <= query_pos[:, None]) & (
-            doc_line[None, :] == documents[:, None]
-        )
-        allowed = allowed[:, None, None, :]
-        scores = jnp.where(allowed, scores, masked_score)
-        new_max = jnp.maximum(running_max, jnp.max(scores, axis=-1))
-        weights = jnp.where(allowed, jnp.exp(scores - new_max[..., None]), 0.0)
-        new_sum = jnp.sum(weights, axis=-1)
-        added = jnp.einsum(
-            "qagk,adk->qagd",
-            weights.astype(jnp.bfloat16),
-            value_block,
-            preferred_element_type=jnp.float32,
-        )
-        return (new_max, new_sum, added)
-
-    active = (jnp.int32(0) <= query_last) & (doc_line[width_keys - 1] >= documents[0])
-    running_max, running_sum, numerator = lax.cond(active, update, lambda state: state, initial)
-    attended = (
-        (numerator / running_sum[..., None])
-        .astype(jnp.bfloat16)
-        .reshape(tok_rows, local_heads * HD)
-    )
+    attended = attend(queries, keys, values, gate_cache, documents)
     token_heads = lax.all_to_all(attended, "tp", split_axis=0, concat_axis=1, tiled=True)
     mixed = jnp.dot(token_heads, out_weight, preferred_element_type=jnp.float32)
     mixed = lax.optimization_barrier(mixed.astype(jnp.bfloat16)).astype(jnp.float32)

time: 394 us -> 295 us (0.75)
  blocking collectives: 180 us -> 125 us
  waiting for transfers between devices: 121 us -> 92.3 us
  between operations: 14.9 us -> 0.21 us
  Pallas kernels: 0 us -> 12.9 us
  matrix products: 40.2 us -> 27.9 us
  other arithmetic: 13.8 us -> 8.62 us
    all_gather x2 -> x0, blocking collectives: 78.8 us -> none  [the longest x1 42.7 us: local(): lax.all_gather(documents.reshape(1, tok_rows), 'sp', axis=1, tiled=True)]
    all_gather x2 -> x0, waiting for transfers between devices: 29.3 us -> none  [the longest x1 29.3 us: local(): value_piece = lax.all_gather(values, 'sp', axis=1, tiled=True)]
    all_to_all x1, blocking collectives: 96.7 us -> 125 us  [local(): lax.all_to_all(outgoing, ('sp', 'tp'), split_axis=0, concat_axis=0, tiled...]
    pallas_call x0 -> x1, Pallas kernels: none -> 12.9 us  [attend(): pl.pallas_call(functools.partial(attend_kernel, planes, across), out_shap...]
    dot_general x2 -> x0, matrix products: 12.3 us -> none  [the longest x1 6.82 us: update(): jnp.einsum('qagk,adk->qagd', weights.astype(jnp.bfloat16), value_block, p...]
    reduce_sum x1 -> x0, other arithmetic: 5.79 us -> none  [update(): new_sum = jnp.sum(weights, axis=-1)]
    all_to_all x1 -> x0, blocking collectives: 3.94 us -> none  [local(): lax.all_to_all(attended, 'tp', split_axis=0, concat_axis=1, tiled=True)]
  transfers between devices with their start and end apart: 3 -> 2, of which waited for: 2 -> 2; matrix products, arithmetic and copies ran while one was open for 2% -> 1% of each run, Pallas kernels for 0% -> 0%
where the time goes in v1:
time: 295 us; the launch traced here: 294 us
  blocking collectives  125 us (42%)
  waiting for transfers between devices  92.3 us (31%)
  matrix products  27.9 us (9%)
  local copies, waits for them, and re-layouts  19.5 us (7%)
  Pallas kernels  12.9 us (4%)
  other arithmetic  8.62 us (3%)
  starting transfers between devices  7.23 us (2%)
    all_to_all x1, blocking collectives, local(): lax.all_to_all(outgoing, ('sp', 'tp'), split_axis=0, concat_axis=0, tiled...  125 us
    all_to_all x1, waiting for transfers between devices, local(): lax.all_to_all(finished, ('sp', 'tp'), split_axis=0, concat_axis=0, tiled...  91.1 us
    pallas_call x1, Pallas kernels, attend(): pl.pallas_call(functools.partial(attend_kernel, planes, across), out_shap...  12.9 us
    gather x2, local copies, waits for them, and re-layouts, local(): jnp.take(returned, slots, axis=0).reshape(row_count, top_count, width_model)  12.1 us
    dot_general x1, matrix products, expert_block(): jnp.einsum('nemf,efd->nemd', hidden, expert_down, preferred_element_type=...  10 us
  transfers between devices with their start and end apart: 2, of which 2 were waited for; matrix products, arithmetic and copies ran while one was open for 1% of the time, Pallas kernels for 0%

profile of v1, /device:TPU:0, one launch (start us, length us, event | category | flops | bytes accessed | tf_op | source)
XLA Modules:
  0.0 293.8 jit_solution(2013004763785808504)
XLA Ops:
  0.0 0.8 convert_element_type.50
  0.8 0.8 copy.37.doc_ref
  1.6 1.5 copy.36
  3.1 1.3 pad_maximum_fusion.1.aux_ref
  4.4 1.5 pad_maximum_fusion.kv_ref
  6.0 12.9 %attend.1 = bf16[256,512]{1,0:T(8,128)(2,1)} custom-call(bf16[256,512]{1,0:T(8,128)(2,1)} %q_ref.1, bf16[256,256]{1,0:T(8,128)(2,1)} %pad_maximum_fusion.kv_ref, f32[8,256]{1,0:T(8,128)} %pad_maximum_fusion.1.aux_ref, f32[256,4]{1,0:T(8,128)} %bitcast.100, f32[256,1]{1,0:T(8,128)} %copy.37.doc_ref), custom_call_target="tpu_custom_call" | custom-call | tf_op jit(solution)/shard_map/attend/pallas_call | solution.py:209
  18.8 1.8 copy.38
  20.6 3.4 %all-to-all-start = ((bf16[2,128,512]{1,2,0:T(8,128)(2,1)}), bf16[2,128,512]{1,2,0:T(8,128)(2,1)S(1)}, u32[]{:S(2)}, u32[]{:S(2)}) async-start(bf16[2,128,512]{1,2,0:T(8,128)(2,1)} %copy.38), calls=%async_computation | async-start | bytes 524288 | tf_op jit(solution)/shard_map/all_to_all | solution.py:263
  24.4 1.2 all-to-all-done
  25.6 3.0 %convolution_convert_fusion.2 = bf16[128,2048]{1,0:T(8,128)(2,1)S(1)} fusion(bf16[128,1024]{0,1:T(8,128)(2,1)S(1)} %bitcast.98, bf16[1024,2048]{1,0:T(8,128)(2,1)} %param.23), kind=kOutput, calls=%fused_computation.4 | convolution fusion | flops 537133056 | bytes 4980736 | tf_op jit(solution)/shard_map/dot_general | solution.py:264
  28.6 0.3 fusion.20
  28.9 0.3 multiply_reduce_fusion.1
  29.3 1.2 reduce-window.6
  30.5 0.2 slice_reduce_fusion
  31.1 0.4 fusion.11
  31.4 1.3 multiply_convert_fusion.1
  32.8 1.2 convolution_convert_fusion.1
  34.0 125.2 %all_to_all.29 = bf16[32,32,2048]{2,1,0:T(8,128)(2,1)S(1)} all-to-all(bf16[32,32,2048]{2,1,0:T(8,128)(2,1)S(1)} %bitcast.97), channel_id=1, replica_groups=mesh['sp'=16,'tp'=2] {'sp','tp'}, dimensions={0} | all-to-all | bytes 8388608 | tf_op jit(solution)/shard_map/all_to_all | solution.py:285
  159.3 2.0 copy-done.3
  161.2 3.7 %fusion.2 = f32[32,32,512]{2,1,0:T(8,128)} fusion(bf16[32,32,2048]{2,1,0:T(8,128)(2,1)S(1)} %all_to_all.29, bf16[1,2048,512]{2,1,0:T(8,128)(2,1)S(1)} %copy-done.8), kind=kOutput, calls=%fused_computation.8 | convolution fusion | flops 2147483648 | bytes 8388608 | tf_op jit(solution)/shard_map/nemd,edf->nemf/dot_general | solution.py:237
  165.0 10.0 %convolution_convert_fusion = bf16[32,32,2048]{2,1,0:T(8,128)(2,1)} fusion(bf16[1,512,2048]{2,1,0:T(8,128)(2,1)S(1)} %copy-done, f32[32,32,512]{2,1,0:T(8,128)} %fusion.2, bf16[32,32,2048]{2,1,0:T(8,128)(2,1)} %copy-done.3, bf16[1,2048,512]{2,1,0:T(8,128)(2,1)} %param.27), kind=kOutput, calls=%fused_computation.1 | convolution fusion | flops 4300210176 | bytes 14680064 | tf_op jit(solution)/shard_map/nemf,efd->nemd/dot_general | solution.py:239
  175.0 3.8 %all-to-all-start.2 = ((bf16[32,32,2048]{2,1,0:T(8,128)(2,1)}), bf16[32,32,2048]{2,1,0:T(8,128)(2,1)}, u32[]{:S(2)}, u32[]{:S(2)}) async-start(bf16[32,32,2048]{2,1,0:T(8,128)(2,1)} %convolution_convert_fusion), calls=%async_computation.2 | async-start | bytes 8388608 | tf_op jit(solution)/shard_map/all_to_all | solution.py:290
  179.1 0.1 copy.43
  179.2 0.2 copy.45
  179.4 2.0 fusion.38
  181.5 91.1 %all-to-all-done.2 = bf16[32,32,2048]{2,1,0:T(8,128)(2,1)} async-done(((bf16[32,32,2048]{2,1,0:T(8,128)(2,1)}), bf16[32,32,2048]{2,1,0:T(8,128)(2,1)}, u32[]{:S(2)}, u32[]{:S(2)}) %all-to-all-start.2) | async-done | bytes 4194336 | tf_op jit(solution)/shard_map/all_to_all | solution.py:290
  272.5 8.0 %gather_fusion = bf16[512,2048]{1,0:T(8,128)(2,1)} fusion(bf16[1024,2048]{1,0:T(8,128)(2,1)} %bitcast.22, s32[1024]{0:T(1024)S(1)} %pad_clamp_fusion), kind=kCustom, calls=%fused_computation | custom fusion | bytes 4196352 | tf_op jit(solution)/shard_map/jit(_take)/gather | solution.py:292
  280.6 4.1 %gather.7 = bf16[128,4,2048]{2,1,0:T(4,128)(2,1)} reshape(bf16[512,2048]{1,0:T(8,128)(2,1)} %gather_fusion) | data formatting | bytes 4194304 | tf_op jit(solution)/shard_map/jit(_take)/gather | solution.py:292
  284.7 3.9 %fusion.9 = f32[128,1,2048]{2,1,0:T(1,128)} fusion(bf16[128,4,1]{1,2,0:T(2,128)(2,1)S(1)} %copy.45, bf16[128,4,2048]{2,1,0:T(4,128)(2,1)} %gather.7, pred[128,4]{1,0:T(8,128)(4,1)S(1)} %copy.43), kind=kOutput, calls=%fused_computation.18 | convolution fusion | flops 3145728 | bytes 3147264 | tf_op jit(solution)/shard_map/rkd,rk->rd/dot_general | solution.py:293
  288.6 4.0 %fusion.37 = (f32[128]{0:T(128)S(1)}, f32[128,2048]{1,0:T(8,128)S(1)}) fusion(bf16[512,2048]{1,0:T(8,128)(2,1)} %param.32, bf16[128,2048]{1,0:T(8,128)(2,1)} %copy-done.1, bf16[2048,512]{1,0:T(8,128)(2,1)} %param.31, f32[128,512]{1,0:T(8,128)S(1)} %fusion.38, f32[128,1,2048]{2,1,0:T(1,128)} %fusion.9), kind=kOutput, calls=%fused_computation.63 | convolution fusion | flops 538574720 | bytes 7078400 | tf_op jit(solution)/shard_map/dot_general | solution.py:297
  292.6 0.3 multiply_reduce_fusion
  292.8 1.0 multiply_convert_fusion
  (40 shorter events, 1.0 us)
Async XLA Ops:
  0.0 165.0 %copy-start = (bf16[1,512,2048]{2,1,0:T(8,128)(2,1)S(1)}, bf16[1,512,2048]{2,1,0:T(8,128)(2,1)}, u32[]{:S(2)}) copy-start(bf16[1,512,2048]{2,1,0:T(8,128)(2,1)} %param.29) | copy-start | bytes 6291460
  0.0 24.1 %copy-start.4 = (s32[128,4]{0,1:T(4,128)S(1)}, s32[128,4]{0,1:T(4,128)}, u32[]{:S(2)}) copy-start(s32[128,4]{0,1:T(4,128)} %param.25) | copy-start | bytes 6148
  20.6 5.0 %all-to-all-start = ((bf16[2,128,512]{1,2,0:T(8,128)(2,1)}), bf16[2,128,512]{1,2,0:T(8,128)(2,1)S(1)}, u32[]{:S(2)}, u32[]{:S(2)}) async-start(bf16[2,128,512]{1,2,0:T(8,128)(2,1)} %copy.38), calls=%async_computation | async-start | bytes 524288 | tf_op jit(solution)/shard_map/all_to_all | solution.py:263
  25.6 3.0 %copy-start.2 = (bf16[128,2048]{1,0:T(8,128)(2,1)S(1)}, bf16[128,2048]{1,0:T(8,128)(2,1)}, u32[]{:S(2)}) copy-start(bf16[128,2048]{1,0:T(8,128)(2,1)} %param.22) | copy-start | bytes 1572868
  28.6 0.7 copy-start.5
  32.8 146.7 %copy-start.1 = (bf16[128,2048]{1,0:T(8,128)(2,1)}, bf16[128,2048]{1,0:T(8,128)(2,1)S(1)}, u32[]{:S(2)}) copy-start(bf16[128,2048]{1,0:T(8,128)(2,1)S(1)} %multiply_convert_fusion.1) | copy-start | bytes 1572868
  34.0 127.2 %copy-start.8 = (bf16[1,2048,512]{2,1,0:T(8,128)(2,1)S(1)}, bf16[1,2048,512]{2,1,0:T(8,128)(2,1)}, u32[]{:S(2)}) copy-start(bf16[1,2048,512]{2,1,0:T(8,128)(2,1)} %param.28) | copy-start | bytes 6291460
  159.3 2.0 copy-start.3
  175.0 4.2 %copy-start.7 = (f32[128,4]{0,1:T(4,128)S(1)}, f32[128,4]{0,1:T(4,128)}, u32[]{:S(2)}) copy-start(f32[128,4]{0,1:T(4,128)} %param.26) | copy-start | bytes 6148
  175.0 4.3 %copy-start.6 = (bf16[2048]{0:T(1024)(128)(2,1)S(1)}, bf16[2048]{0:T(1024)(128)(2,1)}, u32[]{:S(2)}) copy-start(bf16[2048]{0:T(1024)(128)(2,1)} %param.33) | copy-start | bytes 12292
  175.0 97.5 %all-to-all-start.2 = ((bf16[32,32,2048]{2,1,0:T(8,128)(2,1)}), bf16[32,32,2048]{2,1,0:T(8,128)(2,1)}, u32[]{:S(2)}, u32[]{:S(2)}) async-start(bf16[32,32,2048]{2,1,0:T(8,128)(2,1)} %convolution_convert_fusion), calls=%async_computation.2 | async-start | bytes 8388608 | tf_op jit(solution)/shard_map/all_to_all | solution.py:290

commit v2 on v1

--- a/solution.py
+++ b/solution.py
@@ -240,6 +240,387 @@
     return produced.astype(jnp.bfloat16).reshape(arrived.shape)
 
 
+def remote(source, target, send_sem, recv_sem, place, core):
+    return pltpu.make_async_remote_copy(
+        src_ref=source,
+        dst_ref=target,
+        send_sem=send_sem,
+        recv_sem=recv_sem,
+        device_id={"sp": place, "tp": core},
+        device_id_type=pl.DeviceIdType.MESH,
+    )
+
+
+def greet(barrier, place, core):
+    pl.semaphore_signal(
+        barrier,
+        inc=1,
+        device_id={"sp": place, "tp": core},
+        device_id_type=pl.DeviceIdType.MESH,
+    )
+
+
+def slot_matrix(meta, first, rows, top_count, weighted):
+    width = meta.shape[1]
+    row_ids = (first + lax.broadcasted_iota(jnp.int32, (rows, width), 0)).astype(jnp.float32)
+    matrix = jnp.zeros((rows, width), jnp.float32)
+    for choice in range(top_count):
+        filled = meta[top_count + choice : top_count + choice + 1, :] if weighted else 1.0
+        matrix = matrix + jnp.where(row_ids == meta[choice : choice + 1, :], filled, 0.0)
+    return matrix
+
+
+def dispatch_kernel(
+    planes, across, cores, top_count, chunk, rows_ref, meta_ref, arrived_ref, meta_all,
+    blocks, outgoing, own_sem, up_send, up_recv, down_send, down_recv, out_send, out_recv,
+):
+    group = across * cores
+    piece = outgoing.shape[2]
+    width = rows_ref.shape[1]
+    me, core = lax.axis_index("sp"), lax.axis_index("tp")
+    plane, column = me // across, me % across
+    seat = column * cores + core
+
+    barrier = pltpu.get_barrier_semaphore()
+    for offset in range(1, group):
+        other = (seat + offset) % group
+        greet(barrier, plane * across + other // cores, other % cores)
+
+    @pl.when(plane + 1 < planes)
+    def _():
+        greet(barrier, me + across, core)
+
+    @pl.when(plane > 0)
+    def _():
+        greet(barrier, me - across, core)
+
+    peers = group + 1
+    pl.semaphore_wait(barrier, peers - (planes - plane) // planes - (plane + 1) // planes)
+
+    def relay(block, place, send_sem, recv_sem, step):
+        return [
+            remote(
+                ref.at[block], ref.at[block], send_sem.at[step, part], recv_sem.at[step, part],
+                place, core,
+            )
+            for part, ref in enumerate((blocks, meta_all))
+        ]
+
+    def pass_up(block, step):
+        @pl.when(plane + 1 < planes)
+        def _():
+            for copy in relay(block, me + across, up_send, up_recv, step):
+                copy.start()
+
+    def pass_down(block, step):
+        @pl.when(plane > 0)
+        def _():
+            for copy in relay(block, me - across, down_send, down_recv, step):
+                copy.start()
+
+    def piece_copy(block, offset):
+        other = (seat + offset) % group
+        return remote(
+            outgoing.at[block, other],
+            arrived_ref.at[block * group + seat],
+            out_send.at[block, offset],
+            out_recv.at[block, offset],
+            plane * across + other // cores,
+            other % cores,
+        )
+
+    def own_piece(block):
+        return pltpu.make_async_copy(
+            outgoing.at[block, seat], arrived_ref.at[block * group + seat], out_send.at[block, 0]
+        )
+
+    def place_rows(block):
+        matrix = slot_matrix(
+            meta_all[block], plane * group * piece, group * piece, top_count, False
+        ).astype(jnp.bfloat16)
+        for start in range(0, width, chunk):
+            columns = slice(start, start + chunk)
+            placed = jnp.dot(
+                matrix, blocks[block, :, columns], preferred_element_type=jnp.float32
+            )
+            outgoing[block, :, :, columns] = placed.reshape(group, piece, chunk).astype(
+                jnp.bfloat16
+            )
+
+        def start_piece(offset, carry):
+            piece_copy(block, offset).start()
+            return carry
+
+        lax.fori_loop(1, group, start_piece, 0)
+        own_piece(block).start()
+
+    own = [
+        pltpu.make_async_copy(rows_ref, blocks.at[plane], own_sem.at[0]),
+        pltpu.make_async_copy(meta_ref, meta_all.at[plane], own_sem.at[1]),
+    ]
+    for copy in own:
+        copy.start()
+    for copy in own:
+        copy.wait()
+    pass_up(plane, 0)
+    pass_down(plane, 0)
+    place_rows(plane)
+
+    def gather(step, carry):
+        @pl.when(plane >= step)
+        def _():
+            for copy in relay(plane - step, me - across, up_send, up_recv, step - 1):
+                copy.wait_recv()
+            pass_up(plane - step, step)
+
+        @pl.when(plane + step < planes)
+        def _():
+            for copy in relay(plane + step, me + across, down_send, down_recv, step - 1):
+                copy.wait_recv()
+            pass_down(plane + step, step)
+
+        @pl.when(plane >= step)
+        def _():
+            place_rows(plane - step)
+
+        @pl.when(plane + step < planes)
+        def _():
+            place_rows(plane + step)
+
+        return carry
+
+    lax.fori_loop(1, planes, gather, 0)
+
+    def settle(step, carry):
+        @pl.when((plane >= step) & (plane + 1 < planes))
+        def _():
+            for copy in relay(plane - step, me + across, up_send, up_recv, step):
+                copy.wait_send()
+
+        @pl.when((plane + step < planes) & (plane > 0))
+        def _():
+            for copy in relay(plane + step, me - across, down_send, down_recv, step):
+                copy.wait_send()
+
+        own_piece(step).wait()
+
+        def finish_piece(offset, inner):
+            piece_copy(step, offset).wait_send()
+            other = (seat + group - offset) % group
+            remote(
+                outgoing.at[step, other],
+                arrived_ref.at[step * group + other],
+                out_send.at[step, offset],
+                out_recv.at[step, offset],
+                plane * across + other // cores,
+                other % cores,
+            ).wait_recv()
+            return inner
+
+        lax.fori_loop(1, group, finish_piece, 0)
+        return carry
+
+    lax.fori_loop(0, planes, settle, 0)
+
+
+def combine_kernel(
+    planes, across, cores, top_count, chunk, finished_ref, meta_ref, out_ref,
+    back, partial, landed, back_send, back_recv, far_send, far_recv,
+):
+    group = across * cores
+    piece = back.shape[2]
+    width = out_ref.shape[1]
+    me, core = lax.axis_index("sp"), lax.axis_index("tp")
+    plane, column = me // across, me % across
+    seat = column * cores + core
+
+    barrier = pltpu.get_barrier_semaphore()
+    for offset in range(1, group):
+        other = (seat + offset) % group
+        greet(barrier, plane * across + other // cores, other % cores)
+    for offset in range(1, planes):
+        greet(barrier, (plane + offset) % planes * across + column, core)
+    pl.semaphore_wait(barrier, group - 1 + planes - 1)
+
+    def piece_copy(block, offset):
+        other = (seat + offset) % group
+        return remote(
+            finished_ref.at[block * group + other],
+            back.at[block, seat],
+            back_send.at[block, offset],
+            back_recv.at[block, offset],
+            plane * across + other // cores,
+            other % cores,
+        )
+
+    def own_piece(block):
+        return pltpu.make_async_copy(
+            finished_ref.at[block * group + seat], back.at[block, seat], back_send.at[block, 0]
+        )
+
+    def far_copy(turn):
+        block = (plane + turn) % planes
+        return remote(
+            partial.at[block], landed.at[turn], far_send.at[turn], far_recv.at[turn],
+            block * across + column, core,
+        )
+
+    def send_block(turn, carry):
+        block = (plane + turn) % planes
+
+        def start_piece(offset, inner):
+            piece_copy(block, offset).start()
+            return inner
+
+        own_piece(block).start()
+        lax.fori_loop(1, group, start_piece, 0)
+        return carry
+
+    lax.fori_loop(1, planes + 1, send_block, 0)
+
+    def collect(block, store):
+        own_piece(block).wait()
+
+        def wait_piece(offset, inner):
+            other = (seat + group - offset) % group
+            remote(
+                finished_ref.at[block * group + seat],
+                back.at[block, other],
+                back_send.at[block, offset],
+                back_recv.at[block, offset],
+                plane * across + other // cores,
+                other % cores,
+            ).wait_recv()
+            return inner
+
+        lax.fori_loop(1, group, wait_piece, 0)
+        matrix = jnp.transpose(
+            slot_matrix(meta_ref[block], plane * group * piece, group * piece, top_count, True)
+        )
+        high = matrix.astype(jnp.bfloat16)
+        low = (matrix - high.astype(jnp.float32)).astype(jnp.bfloat16)
+        for start in range(0, width, chunk):
+            columns = slice(start, start + chunk)
+            rows = (
+                back[block, :, :, columns]
+                .astype(jnp.float32)
+                .reshape(group * piece, chunk)
+                .astype(jnp.bfloat16)
+            )
+            store(
+                columns,
+                jnp.dot(high, rows, preferred_element_type=jnp.float32)
+                + jnp.dot(low, rows, preferred_element_type=jnp.float32),
+            )
+
+    def far_block(turn, carry):
+        block = (plane + turn) % planes
+
+        def store(columns, summed):
+            partial[block, :, columns] = summed.astype(jnp.bfloat16)
+
+        collect(block, store)
+        far_copy(turn).start()
+        return carry
+
+    lax.fori_loop(1, planes, far_block, 0)
+
+    def store_own(columns, summed):
+        out_ref[:, columns] = summed
+
+    collect(plane, store_own)
+
+    def add_far(turn, carry):
+        far_copy(turn).wait_recv()
+        for start in range(0, width, chunk):
+            columns = slice(start, start + chunk)
+            out_ref[:, columns] += landed[turn, :, columns].astype(jnp.float32)
+        return carry
+
+    lax.fori_loop(1, planes, add_far, 0)
+
+    def settle(block, carry):
+        def finish_piece(offset, inner):
+            piece_copy(block, offset).wait_send()
+            return inner
+
+        lax.fori_loop(1, group, finish_piece, 0)
+        return carry
+
+    lax.fori_loop(0, planes, settle, 0)
+
+    def settle_far(turn, carry):
+        far_copy(turn).wait_send()
+        return carry
+
+    lax.fori_loop(1, planes, settle_far, 0)
+
+
+def expert_exchange(settled, slots, route_weight, capacity, expert_weights):
+    row_count, width_model = settled.shape
+    top_count = route_weight.shape[1]
+    places, cores = lax.axis_size("sp"), lax.axis_size("tp")
+    planes = min(4, places)
+    across = places // planes
+    group = across * cores
+    piece = capacity * expert_weights[0].shape[0]
+    chunk = min(512, width_model)
+    meta_rows = (2 * top_count + 7) // 8 * 8
+    meta = jnp.concatenate(
+        [
+            jnp.transpose(slots.reshape(row_count, top_count)).astype(jnp.float32),
+            jnp.transpose(route_weight),
+            jnp.zeros((meta_rows - 2 * top_count, row_count), jnp.float32),
+        ],
+        axis=0,
+    )
+    vmem = pl.BlockSpec(memory_space=pltpu.VMEM)
+    anywhere = pl.BlockSpec(memory_space=pl.ANY)
+    dma = pltpu.SemaphoreType.DMA
+    arrived, meta_all = pl.pallas_call(
+        functools.partial(dispatch_kernel, planes, across, cores, top_count, chunk),
+        out_shape=(
+            jax.ShapeDtypeStruct((places * cores, piece, width_model), jnp.bfloat16),
+            jax.ShapeDtypeStruct((planes, meta_rows, row_count), jnp.float32),
+        ),
+        in_specs=[vmem, vmem],
+        out_specs=(anywhere, vmem),
+        scratch_shapes=[
+            pltpu.VMEM((planes, row_count, width_model), jnp.bfloat16),
+            pltpu.VMEM((planes, group, piece, width_model), jnp.bfloat16),
+            dma((2,)),
+            dma((planes, 2)),
+            dma((planes, 2)),
+            dma((planes, 2)),
+            dma((planes, 2)),
+            dma((planes, group)),
+            dma((planes, group)),
+        ],
+        compiler_params=pltpu.CompilerParams(collective_id=1, has_side_effects=True),
+        name="dispatch",
+    )(settled, meta)
+    finished = expert_block(
+        arrived.reshape(-1, capacity, width_model), *expert_weights
+    ).reshape(arrived.shape)
+    return pl.pallas_call(
+        functools.partial(combine_kernel, planes, across, cores, top_count, chunk),
+        out_shape=jax.ShapeDtypeStruct((row_count, width_model), jnp.float32),
+        in_specs=[anywhere, vmem],
+        out_specs=vmem,
+        scratch_shapes=[
+            pltpu.VMEM((planes, group, piece, width_model), jnp.bfloat16),
+            pltpu.VMEM((planes, row_count, width_model), jnp.bfloat16),
+            pltpu.VMEM((planes, row_count, width_model), jnp.bfloat16),
+            dma((planes, group)),
+            dma((planes, group)),
+            dma((planes,)),
+            dma((planes,)),
+        ],
+        compiler_params=pltpu.CompilerParams(collective_id=2, has_side_effects=True),
+        name="combine",
+    )(finished, meta_all)
+
+
 def local(
     queries,
     keys,
@@ -265,7 +646,6 @@
     mixed = lax.optimization_barrier(mixed.astype(jnp.bfloat16)).astype(jnp.float32)
     settled = normalize(residual_scale * residual.astype(jnp.float32) + mixed, mix_gain)
     row_count = settled.shape[0]
-    width_model = settled.shape[1]
     top_count = routes.shape[1]
     expert_total = lax.axis_size(("sp", "tp")) * expert_gate.shape[0]
     capacity = row_count * lax.axis_size("tp") * top_count // expert_total
@@ -275,22 +655,9 @@
     ).astype(jnp.int32)
     ranks = jnp.sum(jnp.cumsum(matches, axis=0) * matches, axis=1) - 1
     slots = chosen_experts * capacity + ranks
-    placing = slots[None, :] == jnp.arange(expert_total * capacity, dtype=jnp.int32)[:, None]
-    placing = jnp.any(
-        placing.reshape(expert_total * capacity, row_count, top_count), axis=2
-    ).astype(jnp.bfloat16)
-    outgoing = jnp.dot(placing, settled, preferred_element_type=jnp.float32).astype(jnp.bfloat16)
-    outgoing = outgoing.reshape(expert_total, capacity, width_model)
-    finished = expert_block(
-        lax.all_to_all(outgoing, ("sp", "tp"), split_axis=0, concat_axis=0, tiled=True),
-        expert_gate,
-        expert_up,
-        expert_down,
-    )
-    returned = lax.all_to_all(finished, ("sp", "tp"), split_axis=0, concat_axis=0, tiled=True)
-    returned = returned.reshape(expert_total * capacity, width_model)
-    picked_rows = jnp.take(returned, slots, axis=0).reshape(row_count, top_count, width_model)
-    routed = jnp.einsum("rkd,rk->rd", picked_rows.astype(jnp.float32), route_weight)
+    routed = expert_exchange(
+        settled, slots, route_weight, capacity, (expert_gate, expert_up, expert_down)
+    )
     shared_gate_part = jnp.dot(settled, shared_gate, preferred_element_type=jnp.float32)
     shared_up_part = jnp.dot(settled, shared_up, preferred_element_type=jnp.float32)
     shared_hidden = (jax.nn.silu(shared_gate_part) * shared_up_part).astype(jnp.bfloat16)

time: 295 us -> 201 us (0.68)
  Pallas kernels: 12.9 us -> 156 us
  blocking collectives: 125 us -> 0 us
  waiting for transfers between devices: 92.3 us -> 1.2 us
  local copies, waits for them, and re-layouts: 19.5 us -> 4.92 us
  starting transfers between devices: 7.23 us -> 3.44 us
    pallas_call x0 -> x2, Pallas kernels: none -> 143 us  [the longest x1 81.5 us: expert_exchange(): pl.pallas_call(functools.partial(dispatch_kernel, planes, across, cores,...]
    all_to_all x1 -> x0, blocking collectives: 125 us -> none  [local(): lax.all_to_all(outgoing, ('sp', 'tp'), split_axis=0, concat_axis=0, tiled...]
    all_to_all x1 -> x0, waiting for transfers between devices: 91.1 us -> none  [local(): lax.all_to_all(finished, ('sp', 'tp'), split_axis=0, concat_axis=0, tiled...]
    gather x2 -> x0, local copies, waits for them, and re-layouts: 12.1 us -> none  [local(): jnp.take(returned, slots, axis=0).reshape(row_count, top_count, width_model)]
    dot_general x2 -> x0, matrix products: 5.15 us -> none  [the longest x1 3.91 us: local(): jnp.einsum('rkd,rk->rd', picked_rows.astype(jnp.float32), route_weight)]
    all_to_all x1 -> x0, starting transfers between devices: 3.79 us -> none  [local(): lax.all_to_all(finished, ('sp', 'tp'), split_axis=0, concat_axis=0, tiled...]
  transfers between devices with their start and end apart: 2 -> 1, of which waited for: 2 -> 1; matrix products, arithmetic and copies ran while one was open for 1% -> 0% of each run, Pallas kernels for 0% -> 0%
where the time goes in v2:
time: 201 us; the launch traced here: 199 us
  Pallas kernels  156 us (78%)
  matrix products  25.1 us (12%)
  other arithmetic  8.57 us (4%)
  local copies, waits for them, and re-layouts  4.92 us (2%)
  starting transfers between devices  3.44 us (2%)
    pallas_call x1, Pallas kernels, expert_exchange(): pl.pallas_call(functools.partial(dispatch_kernel, planes, across, cores,...  81.5 us
    pallas_call x1, Pallas kernels, expert_exchange(): pl.pallas_call(functools.partial(combine_kernel, planes, across, cores, t...  61.5 us
    pallas_call x1, Pallas kernels, attend(): pl.pallas_call(functools.partial(attend_kernel, planes, across), out_shap...  12.9 us
    dot_general x1, matrix products, expert_block(): jnp.einsum('nemf,efd->nemd', hidden, expert_down, preferred_element_type=...  10.1 us
    dot_general x1, matrix products, expert_block(): jnp.einsum('nemd,edf->nemf', grouped, expert_up, preferred_element_type=j...  5.9 us
  transfers between devices with their start and end apart: 1, of which 1 were waited for; matrix products, arithmetic and copies ran while one was open for 0% of the time, Pallas kernels for 0%

profile of v2, /device:TPU:0, one launch (start us, length us, event | category | flops | bytes accessed | tf_op | source)
XLA Modules:
  0.0 199.3 jit_solution(10864206733310290339)
XLA Ops:
  0.0 0.8 convert_element_type.51
  0.8 0.8 copy.20.doc_ref
  1.6 1.5 copy.19
  3.1 1.3 pad_maximum_fusion.1.aux_ref
  4.4 1.5 pad_maximum_fusion.kv_ref
  6.0 12.9 %attend.1 = bf16[256,512]{1,0:T(8,128)(2,1)} custom-call(bf16[256,512]{1,0:T(8,128)(2,1)} %q_ref.1, bf16[256,256]{1,0:T(8,128)(2,1)} %pad_maximum_fusion.kv_ref, f32[8,256]{1,0:T(8,128)} %pad_maximum_fusion.1.aux_ref, f32[256,4]{1,0:T(8,128)} %bitcast.90, f32[256,1]{1,0:T(8,128)} %copy.20.doc_ref), custom_call_target="tpu_custom_call" | custom-call | tf_op jit(solution)/shard_map/attend/pallas_call | solution.py:209
  18.8 1.8 copy.21
  20.6 3.4 %all-to-all-start = ((bf16[2,128,512]{1,2,0:T(8,128)(2,1)}), bf16[2,128,512]{1,2,0:T(8,128)(2,1)S(1)}, u32[]{:S(2)}, u32[]{:S(2)}) async-start(bf16[2,128,512]{1,2,0:T(8,128)(2,1)} %copy.21), calls=%async_computation | async-start | bytes 524288 | tf_op jit(solution)/shard_map/all_to_all | solution.py:644
  24.1 0.1 copy.22
  24.2 0.1 eq.29
  24.3 0.1 eq.25
  24.4 1.2 all-to-all-done
  25.6 3.0 %convolution_convert_fusion.1 = bf16[128,2048]{1,0:T(8,128)(2,1)S(1)} fusion(bf16[128,1024]{0,1:T(8,128)(2,1)S(1)} %bitcast.88, bf16[1024,2048]{1,0:T(8,128)(2,1)} %param.23), kind=kOutput, calls=%fused_computation.2 | convolution fusion | flops 537133056 | bytes 4980736 | tf_op jit(solution)/shard_map/dot_general | solution.py:645
  28.6 0.3 fusion.15
  28.9 0.3 multiply_reduce_fusion.1
  29.2 0.1 copy-done.3
  29.3 1.2 reduce-window.6
  30.5 0.2 slice_reduce_fusion
  30.8 0.1 fusion.25
  30.9 0.1 sub.25
  31.0 0.1 copy.25
  31.1 1.1 multiply_convert_fusion.1.rows_ref
  32.2 0.6 pad_maximum_fusion.2.meta_ref
  32.8 81.5 %dispatch.1 = (bf16[32,32,2048]{2,1,0:T(8,128)(2,1)}, f32[4,8,128]{2,1,0:T(8,128)}) custom-call(bf16[128,2048]{1,0:T(8,128)(2,1)} %multiply_convert_fusion.1.rows_ref, f32[8,128]{1,0:T(8,128)} %pad_maximum_fusion.2.meta_ref), custom_call_target="tpu_custom_call" | custom-call | tf_op jit(solution)/shard_map/dispatch/pallas_call | solution.py:580
  114.3 2.3 %fusion.30 = f32[128,512]{1,0:T(8,128)S(1)} fusion(bf16[128,2048]{1,0:T(8,128)(2,1)} %multiply_convert_fusion.1.rows_ref, bf16[2048,512]{1,0:T(8,128)(2,1)} %param.30), kind=kOutput, calls=%fused_computation.50 | convolution fusion | flops 268435456 | bytes 2883584 | tf_op jit(solution)/shard_map/dot_general | solution.py:661
  116.6 0.0 copy-done.6
  116.7 5.9 %fusion.2 = f32[32,32,512]{2,1,0:T(8,128)} fusion(bf16[32,32,2048]{2,1,0:T(8,128)(2,1)} %get-tuple-element.7, bf16[1,2048,512]{2,1,0:T(8,128)(2,1)S(1)} %copy-done.6), kind=kOutput, calls=%fused_computation.6 | convolution fusion | flops 2147483648 | bytes 8388608 | tf_op jit(solution)/shard_map/nemd,edf->nemf/dot_general | solution.py:237
  122.6 10.1 %convolution_convert_fusion.finished_ref = bf16[32,32,2048]{2,1,0:T(8,128)(2,1)} fusion(bf16[1,512,2048]{2,1,0:T(8,128)(2,1)S(1)} %copy-done, f32[32,32,512]{2,1,0:T(8,128)} %fusion.2, bf16[32,32,2048]{2,1,0:T(8,128)(2,1)} %get-tuple-element.7, bf16[1,2048,512]{2,1,0:T(8,128)(2,1)} %param.27), kind=kOutput, calls=%fused_computation | convolution fusion | flops 4300210176 | bytes 14680064 | tf_op jit(solution)/shard_map/nemf,efd->nemd/dot_general | solution.py:239
  132.7 61.5 %combine.1 = f32[128,2048]{1,0:T(8,128)} custom-call(bf16[32,32,2048]{2,1,0:T(8,128)(2,1)} %convolution_convert_fusion.finished_ref, f32[4,8,128]{2,1,0:T(8,128)} %get-tuple-element.8.meta_ref), custom_call_target="tpu_custom_call" | custom-call | tf_op jit(solution)/shard_map/combine/pallas_call | solution.py:605
  194.2 3.8 %fusion.29 = (f32[128]{0:T(128)S(1)}, f32[128,2048]{1,0:T(8,128)S(1)}) fusion(bf16[512,2048]{1,0:T(8,128)(2,1)} %param.32, bf16[128,2048]{1,0:T(8,128)(2,1)} %multiply_convert_fusion.1.rows_ref, bf16[2048,512]{1,0:T(8,128)(2,1)} %param.31, f32[128,512]{1,0:T(8,128)S(1)} %fusion.30, f32[128,2048]{1,0:T(8,128)} %combine.1), kind=kOutput, calls=%fused_computation.49 | convolution fusion | flops 538574720 | bytes 7078400 | tf_op jit(solution)/shard_map/dot_general | solution.py:664
  198.0 0.3 multiply_reduce_fusion
  198.3 1.0 multiply_convert_fusion
  (24 shorter events, 0.1 us)
Async XLA Ops:
  0.0 122.6 %copy-start = (bf16[1,512,2048]{2,1,0:T(8,128)(2,1)S(1)}, bf16[1,512,2048]{2,1,0:T(8,128)(2,1)}, u32[]{:S(2)}) copy-start(bf16[1,512,2048]{2,1,0:T(8,128)(2,1)} %param.29) | copy-start | bytes 6291460
  0.0 24.1 %copy-start.2 = (s32[128,4]{0,1:T(4,128)S(1)}, s32[128,4]{0,1:T(4,128)}, u32[]{:S(2)}) copy-start(s32[128,4]{0,1:T(4,128)} %param.25) | copy-start | bytes 6148
  20.6 5.0 %all-to-all-start = ((bf16[2,128,512]{1,2,0:T(8,128)(2,1)}), bf16[2,128,512]{1,2,0:T(8,128)(2,1)S(1)}, u32[]{:S(2)}, u32[]{:S(2)}) async-start(bf16[2,128,512]{1,2,0:T(8,128)(2,1)} %copy.21), calls=%async_computation | async-start | bytes 524288 | tf_op jit(solution)/shard_map/all_to_all | solution.py:644
  25.6 3.0 %copy-start.1 = (bf16[128,2048]{1,0:T(8,128)(2,1)S(1)}, bf16[128,2048]{1,0:T(8,128)(2,1)}, u32[]{:S(2)}) copy-start(bf16[128,2048]{1,0:T(8,128)(2,1)} %param.22) | copy-start | bytes 1572868
  28.6 0.7 copy-start.3
  28.6 3.5 %copy-start.5 = (f32[128,4]{0,1:T(4,128)S(1)}, f32[128,4]{0,1:T(4,128)}, u32[]{:S(2)}) copy-start(f32[128,4]{0,1:T(4,128)} %param.26) | copy-start | bytes 6148
  114.3 2.4 %copy-start.6 = (bf16[1,2048,512]{2,1,0:T(8,128)(2,1)S(1)}, bf16[1,2048,512]{2,1,0:T(8,128)(2,1)}, u32[]{:S(2)}) copy-start(bf16[1,2048,512]{2,1,0:T(8,128)(2,1)} %param.28) | copy-start | bytes 6291460
  194.2 4.1 %copy-start.4 = (bf16[2048]{0:T(1024)(128)(2,1)S(1)}, bf16[2048]{0:T(1024)(128)(2,1)}, u32[]{:S(2)}) copy-start(bf16[2048]{0:T(1024)(128)(2,1)} %param.33) | copy-start | bytes 12292

commit v3 on v2

--- a/solution.py
+++ b/solution.py
@@ -25,13 +25,13 @@
 
 
 def attend_kernel(
-    planes, across, q_ref, kv_ref, aux_ref, gate_ref, doc_ref, out_ref,
+    planes, across, q_ref, key_ref, value_ref, aux_ref, gate_ref, doc_ref, out_ref,
     kv_all, aux_all, top, total, acc, own_sem, up_send, up_recv, side_send, side_recv,
 ):
     heads = gate_ref.shape[1]
     tok_rows = q_ref.shape[0]
-    group_size = heads // (kv_ref.shape[0] // (2 * HD))
-    kv_rows = kv_ref.shape[0] // 2
+    kv_rows = key_ref.shape[0]
+    group_size = heads // (kv_rows // HD)
     me = lax.axis_index("sp")
     plane = me // across
     column = me % across
@@ -74,7 +74,8 @@
         ]
 
     own = [
-        pltpu.make_async_copy(kv_ref, kv_all.at[me], own_sem.at[0]),
+        pltpu.make_async_copy(key_ref, kv_all.at[me, pl.ds(0, kv_rows)], own_sem.at[0]),
+        pltpu.make_async_copy(value_ref, kv_all.at[me, pl.ds(kv_rows, kv_rows)], own_sem.at[2]),
         pltpu.make_async_copy(aux_ref, aux_all.at[me], own_sem.at[1]),
     ]
     for copy in own:
@@ -101,7 +102,7 @@
             scores = jnp.where(allowed, scores, masked_score)
             old_top = top[head]
             new_top = jnp.maximum(old_top, jnp.max(scores, axis=1, keepdims=True))
-            weights = jnp.where(allowed, jnp.exp(scores - new_top), 0.0)
+            weights = jnp.exp(scores - new_top)
             shrink = jnp.exp(old_top - new_top)
             top[head] = new_top
             total[head] = total[head] * shrink + jnp.sum(weights, axis=1, keepdims=True)
@@ -197,7 +198,6 @@
     across = devices // planes
     aux_rows = (heads + 8) // 8 * 8
     doc_line = documents.astype(jnp.float32)
-    packed = jnp.concatenate([keys, values], axis=0)
     aux = jnp.concatenate(
         [
             gate_cache,
@@ -209,15 +209,15 @@
     return pl.pallas_call(
         functools.partial(attend_kernel, planes, across),
         out_shape=jax.ShapeDtypeStruct((tok_rows, heads * HD), jnp.bfloat16),
-        in_specs=[vmem] * 5,
+        in_specs=[vmem] * 6,
         out_specs=vmem,
         scratch_shapes=[
-            pltpu.VMEM((devices,) + packed.shape, jnp.bfloat16),
+            pltpu.VMEM((devices, 2 * keys.shape[0], tok_rows), jnp.bfloat16),
             pltpu.VMEM((devices,) + aux.shape, jnp.float32),
             pltpu.VMEM((heads, tok_rows, 1), jnp.float32),
             pltpu.VMEM((heads, tok_rows, 1), jnp.float32),
             pltpu.VMEM((tok_rows, heads * HD), jnp.float32),
-            pltpu.SemaphoreType.DMA((2,)),
+            pltpu.SemaphoreType.DMA((3,)),
             pltpu.SemaphoreType.DMA((planes, 2)),
             pltpu.SemaphoreType.DMA((planes, 2)),
             pltpu.SemaphoreType.DMA((planes * across, 2)),
@@ -225,7 +225,7 @@
         ],
         compiler_params=pltpu.CompilerParams(collective_id=0, has_side_effects=True),
         name="attend",
-    )(queries, packed, aux, jnp.transpose(gate_cache), doc_line[:, None])
+    )(queries, keys, values, aux, jnp.transpose(gate_cache), doc_line[:, None])
 
 
 def expert_block(arrived, expert_gate, expert_up, expert_down):

time: 201 us -> 199 us (0.990)
  no operation moved by 1% of the time
where the time goes in v3:
time: 199 us; the launch traced here: 197 us
  Pallas kernels  156 us (78%)
  matrix products  25.1 us (13%)
  other arithmetic  7.04 us (4%)
  local copies, waits for them, and re-layouts  4.92 us (2%)
  starting transfers between devices  3.44 us (2%)
    pallas_call x1, Pallas kernels, expert_exchange(): pl.pallas_call(functools.partial(dispatch_kernel, planes, across, cores,...  81.1 us
    pallas_call x1, Pallas kernels, expert_exchange(): pl.pallas_call(functools.partial(combine_kernel, planes, across, cores, t...  61.5 us
    pallas_call x1, Pallas kernels, attend(): pl.pallas_call(functools.partial(attend_kernel, planes, across), out_shap...  12.9 us
    dot_general x1, matrix products, expert_block(): jnp.einsum('nemf,efd->nemd', hidden, expert_down, preferred_element_type=...  10.1 us
    dot_general x1, matrix products, expert_block(): jnp.einsum('nemd,edf->nemf', grouped, expert_up, preferred_element_type=j...  5.9 us
  transfers between devices with their start and end apart: 1, of which 1 were waited for; matrix products, arithmetic and copies ran while one was open for 0% of the time, Pallas kernels for 0%

profile of v3, /device:TPU:0, one launch (start us, length us, event | category | flops | bytes accessed | tf_op | source)
XLA Modules:
  0.0 197.4 jit_solution(16508324760910403745)
XLA Ops:
  0.0 0.8 convert_element_type.51
  0.8 0.8 copy.20.doc_ref
  1.7 1.5 copy.19
  3.1 1.3 pad_maximum_fusion.aux_ref
  4.4 12.9 %attend.1 = bf16[256,512]{1,0:T(8,128)(2,1)} custom-call(bf16[256,512]{1,0:T(8,128)(2,1)} %q_ref.1, bf16[128,256]{1,0:T(8,128)(2,1)} %key_ref.1, bf16[128,256]{1,0:T(8,128)(2,1)} %value_ref.1, f32[8,256]{1,0:T(8,128)} %pad_maximum_fusion.aux_ref, f32[256,4]{1,0:T(8,128)} %bitcast.90, f32[256,1]{1,0:T(8,128)} %copy.20.doc_ref), custom_call_target="tpu_custom_call" | custom-call | tf_op jit(solution)/shard_map/attend/pallas_call | solution.py:209
  17.3 1.8 copy.21
  19.1 3.4 %all-to-all-start = ((bf16[2,128,512]{1,2,0:T(8,128)(2,1)}), bf16[2,128,512]{1,2,0:T(8,128)(2,1)S(1)}, u32[]{:S(2)}, u32[]{:S(2)}) async-start(bf16[2,128,512]{1,2,0:T(8,128)(2,1)} %copy.21), calls=%async_computation | async-start | bytes 524288 | tf_op jit(solution)/shard_map/all_to_all | solution.py:644
  22.6 0.1 copy.22
  22.7 0.1 eq.29
  22.8 0.1 eq.25
  22.9 1.2 all-to-all-done
  24.1 3.0 %convolution_convert_fusion.1 = bf16[128,2048]{1,0:T(8,128)(2,1)S(1)} fusion(bf16[128,1024]{0,1:T(8,128)(2,1)S(1)} %bitcast.88, bf16[1024,2048]{1,0:T(8,128)(2,1)} %param.23), kind=kOutput, calls=%fused_computation.2 | convolution fusion | flops 537133056 | bytes 4980736 | tf_op jit(solution)/shard_map/dot_general | solution.py:645
  27.1 0.0 copy-start.3
  27.1 0.3 fusion.15
  27.4 0.3 multiply_reduce_fusion.1
  27.7 0.1 copy-done.3
  27.8 1.2 reduce-window.6
  29.0 0.2 slice_reduce_fusion
  29.2 0.1 fusion.25
  29.4 0.1 sub.25
  29.5 0.1 copy.25
  29.6 1.1 multiply_convert_fusion.1.rows_ref
  30.7 0.6 pad_maximum_fusion.1.meta_ref
  31.3 81.1 %dispatch.1 = (bf16[32,32,2048]{2,1,0:T(8,128)(2,1)}, f32[4,8,128]{2,1,0:T(8,128)}) custom-call(bf16[128,2048]{1,0:T(8,128)(2,1)} %multiply_convert_fusion.1.rows_ref, f32[8,128]{1,0:T(8,128)} %pad_maximum_fusion.1.meta_ref), custom_call_target="tpu_custom_call" | custom-call | tf_op jit(solution)/shard_map/dispatch/pallas_call | solution.py:580
  112.4 2.3 %fusion.30 = f32[128,512]{1,0:T(8,128)S(1)} fusion(bf16[128,2048]{1,0:T(8,128)(2,1)} %multiply_convert_fusion.1.rows_ref, bf16[2048,512]{1,0:T(8,128)(2,1)} %param.30), kind=kOutput, calls=%fused_computation.49 | convolution fusion | flops 268435456 | bytes 2883584 | tf_op jit(solution)/shard_map/dot_general | solution.py:661
  114.8 0.0 copy-done.6
  114.8 5.9 %fusion.2 = f32[32,32,512]{2,1,0:T(8,128)} fusion(bf16[32,32,2048]{2,1,0:T(8,128)(2,1)} %get-tuple-element.7, bf16[1,2048,512]{2,1,0:T(8,128)(2,1)S(1)} %copy-done.6), kind=kOutput, calls=%fused_computation.6 | convolution fusion | flops 2147483648 | bytes 8388608 | tf_op jit(solution)/shard_map/nemd,edf->nemf/dot_general | solution.py:237
  120.7 10.1 %convolution_convert_fusion.finished_ref = bf16[32,32,2048]{2,1,0:T(8,128)(2,1)} fusion(bf16[1,512,2048]{2,1,0:T(8,128)(2,1)S(1)} %copy-done, f32[32,32,512]{2,1,0:T(8,128)} %fusion.2, bf16[32,32,2048]{2,1,0:T(8,128)(2,1)} %get-tuple-element.7, bf16[1,2048,512]{2,1,0:T(8,128)(2,1)} %param.27), kind=kOutput, calls=%fused_computation | convolution fusion | flops 4300210176 | bytes 14680064 | tf_op jit(solution)/shard_map/nemf,efd->nemd/dot_general | solution.py:239
  130.8 61.5 %combine.1 = f32[128,2048]{1,0:T(8,128)} custom-call(bf16[32,32,2048]{2,1,0:T(8,128)(2,1)} %convolution_convert_fusion.finished_ref, f32[4,8,128]{2,1,0:T(8,128)} %get-tuple-element.8.meta_ref), custom_call_target="tpu_custom_call" | custom-call | tf_op jit(solution)/shard_map/combine/pallas_call | solution.py:605
  192.4 3.8 %fusion.29 = (f32[128]{0:T(128)S(1)}, f32[128,2048]{1,0:T(8,128)S(1)}) fusion(bf16[512,2048]{1,0:T(8,128)(2,1)} %param.32, bf16[128,2048]{1,0:T(8,128)(2,1)} %multiply_convert_fusion.1.rows_ref, bf16[2048,512]{1,0:T(8,128)(2,1)} %param.31, f32[128,512]{1,0:T(8,128)S(1)} %fusion.30, f32[128,2048]{1,0:T(8,128)} %combine.1), kind=kOutput, calls=%fused_computation.48 | convolution fusion | flops 538574720 | bytes 7078400 | tf_op jit(solution)/shard_map/dot_general | solution.py:664
  196.2 0.3 multiply_reduce_fusion
  196.4 1.0 multiply_convert_fusion
  (23 shorter events, 0.1 us)
Async XLA Ops:
  0.0 120.7 %copy-start = (bf16[1,512,2048]{2,1,0:T(8,128)(2,1)S(1)}, bf16[1,512,2048]{2,1,0:T(8,128)(2,1)}, u32[]{:S(2)}) copy-start(bf16[1,512,2048]{2,1,0:T(8,128)(2,1)} %param.29) | copy-start | bytes 6291460
  0.0 22.6 %copy-start.2 = (s32[128,4]{0,1:T(4,128)S(1)}, s32[128,4]{0,1:T(4,128)}, u32[]{:S(2)}) copy-start(s32[128,4]{0,1:T(4,128)} %param.25) | copy-start | bytes 6148
  19.1 5.0 %all-to-all-start = ((bf16[2,128,512]{1,2,0:T(8,128)(2,1)}), bf16[2,128,512]{1,2,0:T(8,128)(2,1)S(1)}, u32[]{:S(2)}, u32[]{:S(2)}) async-start(bf16[2,128,512]{1,2,0:T(8,128)(2,1)} %copy.21), calls=%async_computation | async-start | bytes 524288 | tf_op jit(solution)/shard_map/all_to_all | solution.py:644
  24.1 3.0 %copy-start.1 = (bf16[128,2048]{1,0:T(8,128)(2,1)S(1)}, bf16[128,2048]{1,0:T(8,128)(2,1)}, u32[]{:S(2)}) copy-start(bf16[128,2048]{1,0:T(8,128)(2,1)} %param.22) | copy-start | bytes 1572868
  27.1 0.7 copy-start.3
  27.1 3.5 %copy-start.5 = (f32[128,4]{0,1:T(4,128)S(1)}, f32[128,4]{0,1:T(4,128)}, u32[]{:S(2)}) copy-start(f32[128,4]{0,1:T(4,128)} %param.26) | copy-start | bytes 6148
  112.4 2.4 %copy-start.6 = (bf16[1,2048,512]{2,1,0:T(8,128)(2,1)S(1)}, bf16[1,2048,512]{2,1,0:T(8,128)(2,1)}, u32[]{:S(2)}) copy-start(bf16[1,2048,512]{2,1,0:T(8,128)(2,1)} %param.28) | copy-start | bytes 6291460
  192.3 4.1 %copy-start.4 = (bf16[2048]{0:T(1024)(128)(2,1)S(1)}, bf16[2048]{0:T(1024)(128)(2,1)}, u32[]{:S(2)}) copy-start(bf16[2048]{0:T(1024)(128)(2,1)} %param.33) | copy-start | bytes 12292
